TPU v7x, 512 devices: a whole 4x4x16 slice. The times are simulated.
512 devices in a mesh: sp: 32 (over z, core), tp: 16 (over y, x).
Axes of the slice: x: 4, y: 4, z: 16, core: 2. Of those that a mesh axis runs over, the one named last changes fastest.
Arguments:
- residual: bfloat16 [4096, 4096], P('sp', 'tp'), may hold values from -46 to 46
- query_small: bfloat16 [4096, 2048], P('sp', 'tp'), may hold values from -6 to 6
- key_narrow_group: bfloat16 [4096, 2048], P('sp', 'tp'), may hold values from -6 to 6
- query_large: bfloat16 [4096, 4096], P('sp', 'tp'), may hold values from -6 to 6
- key_large: bfloat16 [4096, 4096], P('sp', 'tp'), may hold values from -6 to 6
- values: bfloat16 [4096, 2, 2048], P('sp', None, 'tp'), may hold values from -6 to 6
- gates: bfloat16 [4096, 2, 2048], P('sp', None, 'tp'), may hold values from -6 to 6
- log_decay: float32 [4096, 2, 16], P('sp', None, 'tp'), may hold values from -0.65 to 0, as said below
- head_gain: float32 [2, 2048], P(None, 'tp'), may hold values from 0.1 to 1.9
- out_weight: bfloat16 [2, 2048, 4096], P(None, 'sp', 'tp'), may hold values from -0.09375 to 0.09375
- norm_gain: float32 [4096], P('tp'), may hold values from 0.1 to 1.9
- routes: int32 [4096, 2], P('sp'), may hold values from 0 to 31, all different within a row; in each aligned block of 128 rows (0 to 127, 128 to 255, ...) at most 16 rows name the same one
- route_weight: float32 [4096, 2], P('sp'), may hold values from 0.2 to 1
- expert_gate: bfloat16 [32, 4096, 2048], P('sp', None, 'tp'), may hold values from -0.09375 to 0.09375
- expert_up: bfloat16 [32, 4096, 2048], P('sp', None, 'tp'), may hold values from -0.09375 to 0.09375
- expert_down: bfloat16 [32, 2048, 4096], P('sp', None, 'tp'), may hold values from -0.5 to 0.5
Outputs:
- new_stream: bfloat16 [4096, 4096], P('sp', 'tp')
Inputs may be any that keep to these rules, and one draw needn't show every extreme that they name: `routes`: each row names two different experts; in each aligned block of 128 rows no expert is named more than 16 times, a bound that some block reaches. `log_decay`: negative at every position.
All inputs are finite; a program needn't handle non-finite values.
Results may differ from a plain program's by a relative error of at most 0.019.
Values may be sent and summed in bfloat16 or wider, within the bound.
A program may use at most 64 MiB of HBM per device.

v0:
```python
import functools

import jax
import jax.numpy as jnp
from jax import lax
from jax.sharding import Mesh
from jax.sharding import PartitionSpec as P

D = 4096
SP = ("sp_0", "sp_1")
TP = ("tp_0", "tp_1")


EPS = 1e-06
THETA = 10000.0


def neutral_like(array, identity):
    return jax.tree.map(
        lambda a, e: jnp.broadcast_to(jnp.asarray(e, a.dtype), a.shape), array, identity
    )


def gathered_once(array, axis):
    leaves = jax.tree.leaves(array)
    order = sorted(range(len(leaves)), key=lambda k: -leaves[k].size)
    width = (1, *leaves[order[0]].shape)[-1]
    lines = [
        jnp.pad(leaves[k].reshape(-1), (0, -leaves[k].size % width)).reshape(-1, width)
        for k in order
    ]
    both, at, found = (lax.all_gather(jnp.concatenate(lines), axis), 0, {})
    for k, line in zip(order, lines):
        piece = both[:, at : at + len(line)].reshape(len(both), -1)
        found[k] = piece[:, : leaves[k].size].reshape(-1, *leaves[k].shape)
        at += len(line)
    numbers = iter(range(len(leaves)))
    return jax.tree.map(lambda _: found[next(numbers)], array)


def entering_2(array, axes, combine, identity):
    before = start = neutral_like(array, identity)
    so_far = array
    for axis in reversed(axes):
        devices, place = (lax.axis_size(axis), lax.axis_index(axis))
        pieces = gathered_once(so_far, axis)
        inside, so_far = (start, start)
        for k in range(devices):
            passed = k < place
            so_far = combine(so_far, jax.tree.map(lambda part: part[k], pieces))
            inside = jax.tree.map(lambda new, old: jnp.where(passed, new, old), so_far, inside)
        before = combine(inside, before)
    return before


def in_order(blocks, dim):
    lengths = list(blocks.shape[1:])
    lengths[dim] *= blocks.shape[0]
    return jnp.moveaxis(blocks, 0, dim).reshape(lengths)


def from_everyone(array, axis):
    devices = lax.axis_size(axis)
    return lax.all_to_all(
        jnp.broadcast_to(array[None], (devices, *array.shape)), axis, 0, 0, tiled=True
    )


def gathered_copies(array, axis, dim):
    return in_order(from_everyone(array, axis), dim)


def by_axis(array, axes):
    return functools.reduce(lax.psum, axes, array)


def rotate(block, positions):
    half_dim = block.shape[-1] // 2
    inverse = jnp.power(THETA, -jnp.arange(half_dim, dtype=jnp.float32) * 2.0 / block.shape[-1])
    angles = positions[:, None, None] * inverse
    cosine_val, sine_val = (jnp.cos(angles), jnp.sin(angles))
    lower_half, upper_half = (block[..., :half_dim], block[..., half_dim:])
    return jnp.concatenate(
        [
            lower_half * cosine_val - upper_half * sine_val,
            upper_half * cosine_val + lower_half * sine_val,
        ],
        axis=-1,
    )


def block_terms(rot_queries, rot_keys, value_heads, rates):
    count = rates.shape[0]
    decay_sum = jnp.cumsum(rates, axis=0)
    by_head = decay_sum.T
    causal = (jnp.arange(count)[:, None] >= jnp.arange(count)[None, :])[None]
    spread = by_head[:, :, None] - by_head[:, None, :]
    weight = jnp.where(causal, jnp.exp(jnp.where(causal, spread, 0.0)), 0.0)
    scores = jnp.einsum("ihd,jhd->hij", rot_queries, rot_keys, preferred_element_type=jnp.float32)
    weighted = (scores * weight).astype(jnp.bfloat16)
    within = jnp.einsum("hij,jhv->ihv", weighted, value_heads, preferred_element_type=jnp.float32)
    block_end = decay_sum[-1]
    carried = (
        rot_keys.astype(jnp.float32) * jnp.exp(block_end[None, :] - decay_sum)[:, :, None]
    ).astype(jnp.bfloat16)
    update = jnp.einsum("jhd,jhv->hdv", carried, value_heads, preferred_element_type=jnp.float32)
    return (within, decay_sum, jnp.exp(block_end), update)


def final_result(rot_queries, decay_sum, within, state_in, gate_part, gain_part):
    cross_part = (
        jnp.einsum(
            "ihd,hdv->ihv",
            rot_queries.astype(jnp.float32),
            state_in,
            precision=lax.Precision.HIGHEST,
        )
        * jnp.exp(decay_sum)[:, :, None]
    )
    retained = within + cross_part
    scaled = retained * lax.rsqrt(jnp.mean(retained * retained, axis=-1, keepdims=True) + EPS)
    count, head_count, value_size = retained.shape
    gated = jax.nn.silu(gate_part.astype(jnp.float32)).reshape(count, head_count, value_size)
    return (
        (scaled * gain_part.reshape(head_count, value_size) * gated)
        .reshape(count, -1)
        .astype(jnp.bfloat16)
    )


def prepare(queries, keys_in, value_part, positions, head_count):
    row_count = queries.shape[0]
    key_size = queries.shape[1] // head_count
    rot_queries = rotate(
        queries.astype(jnp.float32).reshape(row_count, head_count, key_size), positions
    ).astype(jnp.bfloat16)
    rot_keys = (
        rotate(keys_in.astype(jnp.float32).reshape(row_count, head_count, key_size), positions)
        * key_size ** (-0.5)
    ).astype(jnp.bfloat16)
    value_heads = value_part.reshape(row_count, head_count, value_part.shape[1] // head_count)
    return (rot_queries, rot_keys, value_heads)


def per_device(
    residual,
    query_small,
    key_narrow_group,
    query_large,
    key_large,
    values,
    gates,
    log_decay,
    head_gain,
    out_weight,
    norm_gain,
    routes,
    route_weight,
    expert_gate,
    expert_up,
    expert_down,
):
    row_count = residual.shape[0]
    head_count = log_decay.shape[2]
    positions = (lax.axis_index(SP) * row_count + jnp.arange(row_count, dtype=jnp.int32)).astype(
        jnp.float32
    )
    query_a, key_a, value_a = prepare(
        query_small, key_narrow_group, values[:, 0], positions, head_count
    )
    query_b, key_b, value_b = prepare(query_large, key_large, values[:, 1], positions, head_count)
    within_a, decay_sum_a, fall_a, update_a = block_terms(query_a, key_a, value_a, log_decay[:, 0])
    within_b, decay_sum_b, fall_b, update_b = block_terms(query_b, key_b, value_b, log_decay[:, 1])

    def combine(before_part, after_part):
        return (
            before_part[0] * after_part[0],
            after_part[0][:, None, None] * before_part[1] + after_part[1],
            before_part[2] * after_part[2],
            after_part[2][:, None, None] * before_part[3] + after_part[3],
        )

    identity = (
        jnp.ones_like(fall_a),
        jnp.zeros_like(update_a),
        jnp.ones_like(fall_b),
        jnp.zeros_like(update_b),
    )
    entering = entering_2((fall_a, update_a, fall_b, update_b), SP, combine, identity)
    output_a = final_result(query_a, decay_sum_a, within_a, entering[1], gates[:, 0], head_gain[0])
    output_b = final_result(query_b, decay_sum_b, within_b, entering[3], gates[:, 1], head_gain[1])
    stacked = jnp.stack([output_a, output_b], axis=1)
    gathered = gathered_copies(stacked, TP, 2)
    mixed = jnp.einsum(
        "tgk,gkd->td",
        gathered,
        lax.all_gather(out_weight, SP, axis=1, tiled=True),
        preferred_element_type=jnp.float32,
    ).astype(jnp.bfloat16)
    stream = residual.astype(jnp.float32) + mixed.astype(jnp.float32)
    square_sum = by_axis(jnp.sum(stream * stream, axis=1), TP)
    normed = (stream * lax.rsqrt(square_sum / D + EPS)[:, None] * norm_gain[None, :]).astype(
        jnp.bfloat16
    )
    experts = lax.axis_size(SP)
    capacity = 4 * row_count // experts
    one_hot = (routes[:, :, None] == jnp.arange(experts, dtype=jnp.int32)[None, None, :]).astype(
        jnp.int32
    )
    one_hot = one_hot.reshape(2 * row_count, experts)
    before = jnp.cumsum(one_hot, axis=0) - one_hot
    slot_index = jnp.sum(before * one_hot, axis=1).reshape(row_count, 2)
    target = routes * capacity + slot_index
    slot_ids = jnp.arange(experts * capacity, dtype=jnp.int32)
    choose = target[:, :, None] == slot_ids[None, None, :]
    select = jnp.sum(choose.astype(jnp.int32), axis=1).astype(jnp.bfloat16).T
    w_gate, w_up, w_down = (expert_gate[0], expert_up[0], expert_down[0])
    outgoing = jnp.dot(select, normed, preferred_element_type=jnp.float32).astype(jnp.bfloat16)
    outgoing = outgoing.reshape(experts, capacity, normed.shape[1])
    arrived = lax.all_to_all(outgoing, SP, split_axis=0, concat_axis=0, tiled=True)
    expert_arrived = lax.all_gather(arrived, TP, axis=2, tiled=True)
    gate_part = jnp.einsum(
        "sck,kf->scf", expert_arrived, w_gate, preferred_element_type=jnp.float32
    )
    up_part = jnp.einsum("sck,kf->scf", expert_arrived, w_up, preferred_element_type=jnp.float32)
    hidden = (jax.nn.silu(gate_part) * up_part).astype(jnp.bfloat16)
    expert_out = jnp.einsum(
        "scf,fd->scd", gathered_copies(hidden, TP, 2), w_down, preferred_element_type=jnp.float32
    ).astype(jnp.bfloat16)
    returned = lax.all_to_all(expert_out, SP, split_axis=0, concat_axis=0, tiled=True).reshape(
        experts * capacity, -1
    )
    first_pick = jnp.dot(
        choose[:, 0].astype(jnp.bfloat16), returned, preferred_element_type=jnp.float32
    )
    second_pick = jnp.dot(
        choose[:, 1].astype(jnp.bfloat16), returned, preferred_element_type=jnp.float32
    )
    routed = route_weight[:, 0:1] * first_pick + route_weight[:, 1:2] * second_pick
    return (stream + routed).astype(jnp.bfloat16)


def solution(mesh):
    torus = Mesh(mesh.devices.reshape(16, 2, 4, 4), ("sp_0", "sp_1", "tp_0", "tp_1"))
    placed = (
        P(SP, TP),
        P(SP, TP),
        P(SP, TP),
        P(SP, TP),
        P(SP, TP),
        P(SP, None, TP),
        P(SP, None, TP),
        P(SP, None, TP),
        P(None, TP),
        P(None, SP, TP),
        P(TP),
        P(SP, None),
        P(SP, None),
        P(SP, None, TP),
        P(SP, None, TP),
        P(SP, None, TP),
    )
    return jax.shard_map(
        per_device, mesh=torus, in_specs=placed, out_specs=P(SP, TP), check_vma=False
    )
```

profile of v0, /device:TPU:1, one launch (start us, length us, event | category | flops | bytes accessed | tf_op | source)
XLA Modules:
  0.0 372.4 jit_solution(16960491022823976062)
XLA Ops:
  6.6 0.8 slice_bitcast_fusion.9
  7.6 0.5 slice.522
  8.4 0.2 reduce_window_sum.34
  8.5 0.6 slice.523
  9.3 1.0 fusion.295
  11.7 0.9 bitcast_convert_fusion
  12.6 0.7 fusion.301
  13.2 0.8 bitcast_convert_fusion.2
  14.0 0.6 fusion.300
  14.7 0.3 fusion.287
  15.0 0.3 fusion.291
  15.3 0.3 fusion.102
  15.6 0.3 fusion.200
  15.9 8.6 %all-gather.2 = f32[2,386,128]{2,1,0:T(8,128)S(1)} all-gather(f32[1,386,128]{2,1,0:T(8,128)S(1)} %maximum_bitcast_fusion), channel_id=2, replica_groups=mesh['sp_0'=16,'sp_1'=2,'tp_0'=4,'tp_1'=4] {'sp_1'}, dimensions={0}, use_global_device_ids=true | all-gather | bytes 592896 | tf_op jit(solution)/shard_map/all_gather | solution.py:32
  24.5 0.6 fusion.298
  25.1 0.5 fusion.299
  29.2 0.7 fusion.260
  29.9 0.6 fusion.261
  30.5 0.7 maximum_bitcast_fusion.1
  31.3 0.7 all-gather.8.cloned.1.call-update
  33.6 0.3 convolution_bitcast_fusion.2
  34.0 63.0 %all-gather.12.cloned.1.call-done = f32[16,386,128]{2,1,0:T(8,128)} async-done(((f32[1,386,128]{2,1,0:T(8,128)}), f32[16,386,128]{2,1,0:T(8,128)}) %all-gather.12.cloned.1.call-update) | async-done | bytes 3162128 | tf_op jit(solution)/shard_map/all_gather | solution.py:32
  97.0 0.9 fusion.292
  97.9 0.7 fusion.296
  99.1 0.7 fusion.297
  100.4 11.6 %fusion.16 = f32[1,128,128]{2,1,0:T(8,128)S(1)} fusion(f32[16,386,128]{2,1,0:T(8,128)} %all-gather.12.cloned.1.call-done, f32[2,386,128]{2,1,0:T(8,128)S(1)} %all-gather.2, f32[128]{0:T(128)S(1)} %get-tuple-element.71, f32[]{:T(128)} %bitcast.63, f32[]{:T(128)} %bitcast.62, f32[]{:T(128)} %bitcast.61, f32[]{:T(128)} %bitcast.60, f32[]{:T(128)} %bitcast.59, ...), kind=kOutput, calls=%fused_computation.25 | convolution fusion | flops 26132480 | bytes 1322000 | tf_op jit(solution)/shard_map/ihd,hdv->ihv/dot_general | solution.py:112
  111.9 0.4 multiply_reduce_fusion.2
  112.3 12.2 %multiply_reduce_fusion.1 = (f32[128]{0:T(128)S(1)}, f32[1,128,128]{2,1,0:T(8,128)S(1)}) fusion(f32[1,128,128]{2,1,0:T(8,128)S(1)} %convolution_bitcast_fusion.2, f32[128]{0:T(128)S(1)} %get-tuple-element.73, bf16[128,128]{1,0:T(8,128)(2,1)S(1)} %get-tuple-element.67, bf16[128,128]{1,0:T(8,128)(2,1)S(1)} %get-tuple-element.68, ...), kind=kOutput, calls=%fused_computation.180 | convolution fusion | flops 52297600 | bytes 2567696 | tf_op jit(solution)/shard_map/ihd,hdv->ihv/dot_general | solution.py:112
  124.9 1.2 broadcast_in_dim.18
  126.1 6.7 %all-to-all-start = ((bf16[16,128,2,128]{3,1,2,0:T(8,128)(2,1)}), bf16[16,128,2,128]{3,1,2,0:T(8,128)(2,1)S(1)}, u32[]{:S(2)}, u32[]{:S(2)}) async-start(bf16[16,128,2,128]{3,1,2,0:T(8,128)(2,1)} %broadcast_in_dim.18), calls=%async_computation | async-start | bytes 2097152 | tf_op jit(solution)/shard_map/all_to_all | solution.py:64
  133.3 0.6 reduce-window.6
  133.9 0.2 slice_reduce_fusion
  134.5 42.4 %all-gather.8.cloned.1.call-done = bf16[2,2048,256]{2,1,0:T(8,128)(2,1)} async-done(((bf16[2,64,256]{2,1,0:T(8,128)(2,1)}), bf16[2,2048,256]{2,1,0:T(8,128)(2,1)}) %all-gather.8.cloned.1.call-update) | async-done | bytes 2097168 | tf_op jit(solution)/shard_map/all_gather | solution.py:197
  177.0 2.2 multiply_reduce_fusion
  179.1 8.3 %psum.14 = f32[128]{0:T(128)S(1)} all-reduce(f32[128]{0:T(128)S(1)} %get-tuple-element.79), channel_id=1, replica_groups=mesh['sp_0'=16,'sp_1'=2,'tp_0'=4,'tp_1'=4] {'tp_0'}, use_global_device_ids=true, to_apply=%region_9.10 | all-reduce | flops 128 | bytes 1024 | tf_op jit(solution)/shard_map/psum | solution.py:74
  187.4 8.4 %psum.15 = f32[128]{0:T(128)S(1)} all-reduce(f32[128]{0:T(128)S(1)} %psum.14), channel_id=1, replica_groups=mesh['sp_0'=16,'sp_1'=2,'tp_0'=4,'tp_1'=4] {'tp_1'}, use_global_device_ids=true, to_apply=%region_10.11 | all-reduce | flops 128 | bytes 1024 | tf_op jit(solution)/shard_map/psum | solution.py:74
  195.9 0.3 convolution_convert_fusion
  196.2 34.8 %all_to_all.20 = bf16[32,16,256]{2,1,0:T(8,128)(2,1)} all-to-all(bf16[32,16,256]{2,1,0:T(8,128)(2,1)S(1)} %bitcast.244), channel_id=1, replica_groups=mesh['sp_0'=16,'sp_1'=2,'tp_0'=4,'tp_1'=4] {'sp_0','sp_1'}, dimensions={0} | all-to-all | bytes 524288 | tf_op jit(solution)/shard_map/all_to_all | solution.py:220
  231.0 57.7 %all-gather.10.cloned.1.call-done = bf16[32,16,4096]{2,1,0:T(8,128)(2,1)} async-done(((bf16[32,16,256]{2,1,0:T(8,128)(2,1)}), bf16[32,16,4096]{2,1,0:T(8,128)(2,1)}) %all-gather.10.cloned.1.call-update) | async-done | bytes 4194320 | tf_op jit(solution)/shard_map/all_gather | solution.py:221
  288.7 3.6 fusion.23
  292.3 1.3 fusion.6
  293.6 0.4 broadcast_in_dim.19
  294.0 31.7 %all_to_all.21 = bf16[16,32,16,128]{3,2,1,0:T(8,128)(2,1)S(1)} all-to-all(bf16[16,32,16,128]{3,2,1,0:T(8,128)(2,1)S(1)} %broadcast_in_dim.19), channel_id=1, replica_groups=mesh['sp_0'=16,'sp_1'=2,'tp_0'=4,'tp_1'=4] {'tp_0','tp_1'}, dimensions={0} | all-to-all | bytes 4194304 | tf_op jit(solution)/shard_map/all_to_all | solution.py:64
  325.7 1.4 fusion.3
  327.1 15.5 %all-to-all-start.3 = ((bf16[32,16,256]{2,1,0:T(8,128)(2,1)}), bf16[32,16,256]{2,1,0:T(8,128)(2,1)S(1)}, u32[]{:S(2)}, u32[]{:S(2)}) async-start(bf16[32,16,256]{2,1,0:T(8,128)(2,1)} %fusion.3), calls=%async_computation.3 | async-start | bytes 524288 | tf_op jit(solution)/shard_map/all_to_all | solution.py:230
  342.7 22.1 %all-to-all-done.3 = bf16[32,16,256]{2,1,0:T(8,128)(2,1)S(1)} async-done(((bf16[32,16,256]{2,1,0:T(8,128)(2,1)}), bf16[32,16,256]{2,1,0:T(8,128)(2,1)S(1)}, u32[]{:S(2)}, u32[]{:S(2)}) %all-to-all-start.3) | async-done | bytes 262176 | tf_op jit(solution)/shard_map/all_to_all | solution.py:230
  364.8 0.2 convolution_multiply_fusion.2
  365.0 0.8 fusion.9
  (61 shorter events, 2.5 us)
Async XLA Ops:
  6.5 319.1 %copy-start = (bf16[1,2048,256]{2,1,0:T(8,128)(2,1)S(1)}, bf16[1,2048,256]{2,1,0:T(8,128)(2,1)}, u32[]{:S(2)}) copy-start(bf16[1,2048,256]{2,1,0:T(8,128)(2,1)} %param.31) | copy-start | bytes 3145732
  6.5 26.7 %copy-start.3 = (bf16[128,2,128]{2,1,0:T(2,128)(2,1)S(1)}, bf16[128,2,128]{2,1,0:T(2,128)(2,1)}, u32[]{:S(2)}) copy-start(bf16[128,2,128]{2,1,0:T(2,128)(2,1)} %param.22) | copy-start | bytes 196612
  6.5 27.4 %copy-start.6 = (f32[2,128]{1,0:T(2,128)S(1)}, f32[2,128]{1,0:T(2,128)}, u32[]{:S(2)}) copy-start(f32[2,128]{1,0:T(2,128)} %param.24) | copy-start | bytes 3076
  6.5 90.4 %all-gather.12.cloned.1.call-start = ((), (), s32[]{:S(2)}) async-start(), calls=%async_computation.6 | async-start | bytes 3411968 | tf_op jit(solution)/shard_map/all_gather | solution.py:32
  31.3 145.7 %all-gather.8.cloned.1.call-start = ((), (), s32[]{:S(2)}) async-start(), calls=%async_computation.4 | async-start | bytes 2162688 | tf_op jit(solution)/shard_map/all_gather | solution.py:197
  112.3 20.5 %copy-start.4 = (s32[128,2]{0,1:T(2,128)S(1)}, s32[128,2]{0,1:T(2,128)}, u32[]{:S(2)}) copy-start(s32[128,2]{0,1:T(2,128)} %param.27) | copy-start | bytes 3076
  126.1 69.8 %copy-start.5 = (f32[256]{0:T(256)S(1)}, f32[256]{0:T(256)}, u32[]{:S(2)}) copy-start(f32[256]{0:T(256)} %param.26) | copy-start | bytes 3076
  126.1 50.8 %all-to-all-start = ((bf16[16,128,2,128]{3,1,2,0:T(8,128)(2,1)}), bf16[16,128,2,128]{3,1,2,0:T(8,128)(2,1)S(1)}, u32[]{:S(2)}, u32[]{:S(2)}) async-start(bf16[16,128,2,128]{3,1,2,0:T(8,128)(2,1)} %broadcast_in_dim.18), calls=%async_computation | async-start | bytes 2097152 | tf_op jit(solution)/shard_map/all_to_all | solution.py:64
  132.8 155.9 %copy-start.2 = (bf16[1,4096,128]{2,1,0:T(8,128)(2,1)S(1)}, bf16[1,4096,128]{2,1,0:T(8,128)(2,1)}, u32[]{:S(2)}) copy-start(bf16[1,4096,128]{2,1,0:T(8,128)(2,1)} %param.29) | copy-start | bytes 3145732
  132.8 155.9 %all-gather.10.cloned.1.call-start = ((), (), s32[]{:S(2)}) async-start(), calls=%async_computation.5 | async-start | bytes 4456448 | tf_op jit(solution)/shard_map/all_gather | solution.py:221
  196.2 96.1 %copy-start.8 = (bf16[1,4096,128]{2,1,0:T(8,128)(2,1)S(1)}, bf16[1,4096,128]{2,1,0:T(8,128)(2,1)}, u32[]{:S(2)}) copy-start(bf16[1,4096,128]{2,1,0:T(8,128)(2,1)} %param.30) | copy-start | bytes 3145732
  288.7 3.6 copy-start.1
  325.7 16.9 %copy-start.7 = (f32[128,2]{0,1:T(2,128)S(1)}, f32[128,2]{0,1:T(2,128)}, u32[]{:S(2)}) copy-start(f32[128,2]{0,1:T(2,128)} %param.28) | copy-start | bytes 3076
  327.1 37.7 %all-to-all-start.3 = ((bf16[32,16,256]{2,1,0:T(8,128)(2,1)}), bf16[32,16,256]{2,1,0:T(8,128)(2,1)S(1)}, u32[]{:S(2)}, u32[]{:S(2)}) async-start(bf16[32,16,256]{2,1,0:T(8,128)(2,1)} %fusion.3), calls=%async_computation.3 | async-start | bytes 524288 | tf_op jit(solution)/shard_map/all_to_all | solution.py:230
Sparse Core Ops, SparseCore 0:
  31.4 65.5 all-gather.11
  99.1 77.7 all-gather.7
  231.1 57.5 all-gather.9
where the time goes:
time: 374 us; the launch traced here: 372 us
  waiting for transfers between devices  186 us (50%)
  blocking collectives  91.8 us (25%)
  matrix products  34.7 us (9%)
  starting transfers between devices  22.2 us (6%)
  between operations  20.9 us (6%)
  local copies, waits for them, and re-layouts  9.36 us (3%)
  other arithmetic  7.46 us (2%)
    all_gather x1, waiting for transfers between devices, gathered_once(): both, at, found = (lax.all_gather(jnp.concatenate(lines), axis), 0, {})  63 us
    all_gather x1, waiting for transfers between devices, per_device(): expert_arrived = lax.all_gather(arrived, TP, axis=2, tiled=True)  57.7 us
    all_gather x1, waiting for transfers between devices, per_device(): lax.all_gather(out_weight, SP, axis=1, tiled=True)  42.4 us
    all_to_all x1, blocking collectives, per_device(): lax.all_to_all(outgoing, SP, split_axis=0, concat_axis=0, tiled=True)  34.8 us
    all_to_all x1, blocking collectives, from_everyone(): lax.all_to_all(jnp.broadcast_to(array[None], (devices, *array.shape)), ax...  31.7 us
    dot_general x2, matrix products, final_result(): jnp.einsum('ihd,hdv->ihv', rot_queries.astype(jnp.float32), state_in, pre...  23.7 us
    all_to_all x1, waiting for transfers between devices, per_device(): lax.all_to_all(expert_out, SP, split_axis=0, concat_axis=0, tiled=True)  22.1 us
    psum x2, blocking collectives, by_axis(): return functools.reduce(lax.psum, axes, array)  16.8 us
  transfers between devices with their start and end apart: 5, of which 4 were waited for; matrix products, arithmetic and copies ran while one was open for 8% of the time, Pallas kernels for 0%

commit v1 on v0

v1 whole, which is shorter than its diff:
```python
import jax
import jax.numpy as jnp
import numpy as np
from jax import lax
from jax.experimental import pallas as pl
from jax.experimental.pallas import tpu as pltpu
from jax.sharding import PartitionSpec as P

MESH = pl.DeviceIdType.MESH
BF = jnp.bfloat16
F32 = jnp.float32
EPS = 1e-06
THETA = 10000.0
D = 4096
NS, NT, NZ = 32, 16, 16
TOK = 128
NCH = 4
ROWS = NS * 16 // NCH
ORDER = [0, 1, -1, 2, 8, 7, -7, 6, -6, 5, -5, 4, -4, 3, -3, -2]
FAR_FIRST = [8, 7, -7, 6, -6, 5, -5, 4, -4, 3, -3, 2, -2, 1, -1, 0]


def dot(a, b, dims=((1,), (0,)), precision=None):
    return lax.dot_general(a, b, (dims, ((), ())), precision=precision, preferred_element_type=F32)


def silu(v):
    return v / (1.0 + jnp.exp(-v))


def tables():
    i = np.arange(TOK, dtype=np.float64)[:, None]
    s = np.arange(NS, dtype=np.float64)[:, None] * TOK
    small = THETA ** (-np.arange(64, dtype=np.float64) * 2.0 / 128)
    small = np.concatenate([small, small])[None]
    large = THETA ** (-np.arange(128, dtype=np.float64) * 2.0 / 256)[None]

    def four(p):
        return np.concatenate(
            [np.cos(p * small), np.sin(p * small), np.cos(p * large), np.sin(p * large)], axis=1
        ).astype(np.float32)

    return four(i), four(s)[:, None, :]


def kernel(
    res, qs, ks, ql, kl, vals, gates, ld, hgain, wo_in, ngain, routes, rw, wg, wu, wd, tab_i, tab_s,
    out,
    u_send, u_recv, e_send, e_recv, wo, ho, ss_send, ss_recv, stream, choose, xs, x4, wgu, wd2,
    psend, precv, hid, p2send, p2recv, rsend, ret, qa, qb, within,
    ring_sem, part_sem, u_sem, e_sem, c_sem, ss_sem, x_sem, g_sem, m_sem, a_sem, d_sem, r_sem,
    w_sem, loc_sem, snd,
):
    me_s = lax.axis_index("sp")
    me_t = lax.axis_index("tp")
    z, c = lax.div(me_s, 2), lax.rem(me_s, 2)
    y, x = lax.div(me_t, 4), lax.rem(me_t, 4)

    def at_z(dz, j):
        return lax.rem(z + (dz + NZ), NZ) * 2 + lax.rem(c + j, 2)

    def t_of(yy, xx):
        return yy * 4 + xx

    def y_peer(i):
        return lax.rem(y + i, 4)

    def x_peer(i):
        return lax.rem(x + i, 4)

    def send(src, dst, s_sem, r_sem_, s, t):
        pltpu.make_async_remote_copy(
            src_ref=src, dst_ref=dst, send_sem=s_sem, recv_sem=r_sem_, device_id=(s, t), device_id_type=MESH
        ).start()

    def wait(ref, sem):
        pltpu.make_async_copy(ref, ref, sem).wait()

    def lanes(index, size):
        return pl.ds(pl.multiple_of(index * size, size), size)

    barrier = pltpu.get_barrier_semaphore()

    def greet_s(i, carry):
        pl.semaphore_signal(barrier, inc=1, device_id=(lax.rem(me_s + i, NS), me_t), device_id_type=MESH)
        return carry

    def greet_t(i, carry):
        pl.semaphore_signal(barrier, inc=1, device_id=(me_s, lax.rem(me_t + i, NT)), device_id_type=MESH)
        return carry

    lax.fori_loop(1, NS, greet_s, 0)
    lax.fori_loop(1, NT, greet_t, 0)

    local = [
        pltpu.make_async_copy(wg.at[lanes(y, 1024), :], wgu.at[:, lanes(2 * y, 128)], loc_sem.at[0]),
        pltpu.make_async_copy(wu.at[lanes(y, 1024), :], wgu.at[:, lanes(2 * y + 1, 128)], loc_sem.at[1]),
        pltpu.make_async_copy(wd.at[:, x], wd2.at[:, :, lanes(x, 256)], loc_sem.at[2]),
    ]
    for copy in local:
        copy.start()

    row = lax.broadcasted_iota(jnp.int32, (TOK, TOK), 0)
    col = lax.broadcasted_iota(jnp.int32, (TOK, TOK), 1)
    causal = row >= col
    tri = causal.astype(F32)

    def cumul_of(g):
        rates = jnp.broadcast_to(ld[:, g : g + 1], (TOK, TOK))
        return dot(tri, rates, precision=lax.Precision.HIGHEST)

    cum = [cumul_of(0), cumul_of(1)]

    base = tab_s[me_s]

    def turned(k):
        ci, si = tab_i[:, k * 256 : k * 256 + 128], tab_i[:, k * 256 + 128 : k * 256 + 256]
        cs, sn = base[:, k * 256 : k * 256 + 128], base[:, k * 256 + 128 : k * 256 + 256]
        return ci * cs - si * sn, si * cs + ci * sn

    cos_a, sin_a = turned(0)
    cos_b, sin_b = turned(1)
    sin_a = jnp.where(col < 64, -sin_a, sin_a)

    def rot_a(v):
        v = v.astype(F32)
        return v * cos_a + pltpu.roll(v, 64, 1) * sin_a

    def rot_b(v):
        lo, hi = v[:, :128].astype(F32), v[:, 128:].astype(F32)
        return jnp.concatenate([lo * cos_b - hi * sin_b, hi * cos_b + lo * sin_b], axis=1)

    key_a = (rot_a(ks[...]) * (128.0 ** -0.5)).astype(BF)
    key_b = (rot_b(kl[...]) * (256.0 ** -0.5)).astype(BF)
    query_a = rot_a(qs[...]).astype(BF)
    query_b = rot_b(ql[...]).astype(BF)
    value = [vals[:, :128], vals[:, 128:]]

    def spread_to(rows_, width, first):
        d = lax.broadcasted_iota(jnp.int32, (rows_, 512), 0)
        place = lax.broadcasted_iota(jnp.int32, (rows_, 512), 1)
        inner = lax.rem(place, 16) - first
        hit = (inner >= 0) & (inner < width) & (d == lax.div(place, 16) * width + inner)
        return jnp.where(hit, 1.0, 0.0).astype(BF)

    perm_a = spread_to(128, 4, 8)
    perm_b = spread_to(256, 8, 0)

    fall_a = jnp.exp(cum[0][TOK - 1 :, :] - cum[0])
    fall_b = jnp.exp(cum[1][TOK - 1 :, :] - cum[1])
    carried_a = (key_a.astype(F32) * fall_a).astype(BF)
    carried_b = (key_b.astype(F32) * jnp.concatenate([fall_b, fall_b], axis=1)).astype(BF)
    update = dot(dot(carried_a, perm_a).astype(BF), value[0], ((0,), (0,))) + dot(
        dot(carried_b, perm_b).astype(BF), value[1], ((0,), (0,))
    )
    place = lax.rem(lax.broadcasted_iota(jnp.int32, (512, TOK), 0), 16)
    for g, at in ((1, 12), (0, 14)):
        last = cum[g][TOK - 1 :, :]
        high = last.astype(BF).astype(F32)
        update = jnp.where(place == at, high, update)
        update = jnp.where(place == at + 1, last - high, update)
    u_send[...] = update.astype(BF).reshape(NS, 16, TOK)

    pl.semaphore_wait(barrier, NS - 1 + NT - 1)

    def scatter(src, dst, sems):
        for dz in FAR_FIRST:
            for j in (0, 1):
                if dz == 0 and j == 0:
                    continue
                to = at_z(dz, j)
                send(src.at[to], dst.at[me_s], sems.at[0], sems.at[1], to, me_t)
        dst[pl.ds(me_s, 1)] = src[pl.ds(me_s, 1)]

    scatter(u_send, u_recv, u_sem)

    partner = z * 2 + (1 - c)

    def block_of(zz, cc, g):
        head = zz if g == 0 else lax.rem(zz, 4) * 4 + lax.div(zz, 4)
        return wo.at[g, pl.ds(pl.multiple_of(head * 128 + cc * 64, 64), 64), :]

    def ring_send(k):
        for g in (0, 1):
            for way, dz in ((0, 1), (1, -1)):
                if k > 1 and way == 1 and k - 1 > 7:
                    continue
                owner = lax.rem(z - dz * (k - 1) + NZ, NZ)
                block = block_of(owner, c, g)
                src = wo_in.at[g] if k == 1 else block
                if (way == 0 and k <= 8) or (way == 1 and k <= 7):
                    send(src, block, snd.at[0], ring_sem.at[way, k - 1, g], at_z(dz, 0), me_t)
                if k > 1 or way == 0:
                    send(src, block, snd.at[0], part_sem.at[0], partner, me_t)

    def ring_recv(k):
        for g in (0, 1):
            wait(wo_in.at[g], ring_sem.at[0, k - 1, g])
            if k <= 7:
                wait(wo_in.at[g], ring_sem.at[1, k - 1, g])

    def ring_step(k):
        ring_recv(k)
        ring_send(k + 1)

    own = [pltpu.make_async_copy(wo_in.at[g], block_of(z, c, g), loc_sem.at[3 + g]) for g in (0, 1)]
    for copy in own:
        copy.start()
    ring_send(1)

    def spread_weight(src, half):
        for i in (2, 1, 3):
            to = y_peer(i)
            send(src.at[lanes(to, 1024), :], wgu.at[:, lanes(2 * y + half, 128)], w_sem.at[half],
                 w_sem.at[2 + half], me_s, t_of(to, x))

    for i in (2, 1, 3):
        to = x_peer(i)
        send(wd.at[:, to], wd2.at[:, :, lanes(x, 256)], w_sem.at[4], w_sem.at[5], me_s, t_of(y, to))
    spread_weight(wg, 0)

    qa[...] = dot(query_a, perm_a).astype(BF)
    qb[...] = dot(query_b, perm_b).astype(BF)
    for g, (q, k) in enumerate(((query_a, key_a), (query_b, key_b))):
        apart = jnp.where(causal, cum[g] - cum[g].T, 0.0)
        weight = jnp.where(causal, jnp.exp(apart), 0.0)
        weighted = (dot(q, k, ((1,), (1,))) * weight).astype(BF)
        within[g] = dot(weighted, value[g])

    experts = lax.broadcasted_iota(jnp.int32, (TOK, TOK), 1)
    hot = [(routes[:, n : n + 1] == experts).astype(F32) for n in (0, 1)]
    strict = (row > col).astype(BF)
    before = dot(strict, (hot[0] + hot[1]).astype(BF))
    slots = lax.broadcasted_iota(jnp.int32, (TOK, 512), 1)
    for n in (0, 1):
        slot = jnp.sum(before * hot[n], axis=1, keepdims=True).astype(jnp.int32)
        target = routes[:, n : n + 1] * 16 + slot
        choose[n] = jnp.where(slots == target, 1.0, 0.0).astype(BF)

    for k in (1, 2):
        ring_step(k)

    wait(u_recv.at[0 : NS - 1], u_sem.at[1])
    state = jnp.zeros((16, TOK), F32)
    first_rows = lax.broadcasted_iota(jnp.int32, (16, TOK), 0) < 8
    for s in range(NS):
        e_send[s] = state.astype(BF)
        if s < NS - 1:
            piece = u_recv[s].astype(F32)
            drop_b = jnp.exp(piece[12:13] + piece[13:14])
            drop_a = jnp.exp(piece[14:15] + piece[15:16])
            state = jnp.where(first_rows, drop_b, drop_a) * state + piece
    scatter(e_send, e_recv, e_sem)

    for k in (3, 4, 5):
        ring_step(k)

    wait(e_recv.at[0 : NS - 1], e_sem.at[1])
    entering = e_recv[...].reshape(512, TOK)
    spots = (me_t, x * 4 + y)
    for g, q in ((0, qa), (1, qb)):
        retained = within[g] + jnp.exp(cum[g]) * dot(q[...], entering)
        scaled = retained * lax.rsqrt(jnp.mean(retained * retained, axis=1, keepdims=True) + EPS)
        gate = gates[:, g * 128 : (g + 1) * 128].astype(F32)
        ho[g, :, lanes(spots[g], 128)] = (scaled * hgain[g : g + 1, :] * silu(gate)).astype(BF)

    for i in (2, 1, 3):
        mine = ho.at[0, :, lanes(spots[0], 128)]
        send(mine, mine, snd.at[1], c_sem.at[0], me_s, t_of(y, x_peer(i)))
        mine = ho.at[1, :, lanes(spots[1], 128)]
        send(mine, mine, snd.at[1], c_sem.at[1], me_s, t_of(y_peer(i), x))
    ring_step(6)
    wait(ho.at[0, :, 0:384], c_sem.at[0])
    for i in (2, 1, 3):
        mine = ho.at[0, :, lanes(y, 512)]
        send(mine, mine, snd.at[2], c_sem.at[2], me_s, t_of(y_peer(i), x))
    wait(ho.at[1, :, 0:384], c_sem.at[1])
    for i in (2, 1, 3):
        mine = ho.at[1, :, lanes(x, 512)]
        send(mine, mine, snd.at[2], c_sem.at[3], me_s, t_of(y, x_peer(i)))
    ring_step(7)
    ring_recv(8)
    for g in (0, 1):
        block = block_of(lax.rem(z + 8, NZ), c, g)
        send(block, block, snd.at[0], part_sem.at[0], partner, me_t)
    for copy in own:
        copy.wait()
    wait(wo.at[0], part_sem.at[0])
    wait(ho.at[0, :, 0:1536], c_sem.at[2])
    mixed = dot(ho[0], wo[0])
    wait(ho.at[1, :, 0:1536], c_sem.at[3])
    mixed = mixed + dot(ho[1], wo[1])
    now = res[...].astype(F32) + mixed.astype(BF).astype(F32)
    stream[...] = now
    squares = jnp.sum(now * now, axis=1, keepdims=True)
    line = jnp.broadcast_to(squares, (TOK, TOK)).T[0:1, :]
    ss_send[...] = line
    ss_recv[me_t] = line
    for i in (10, 9, 11, 5, 6, 7, 13, 14, 15, 2, 8, 1, 3, 4, 12):
        send(ss_send, ss_recv.at[me_t], snd.at[3], ss_sem.at[0], me_s, lax.rem(me_t + i, NT))
    spread_weight(wu, 1)
    wait(ss_recv.at[0 : NT - 1], ss_sem.at[0])
    total = jnp.sum(ss_recv[...], axis=0)
    total = jnp.broadcast_to(total, (TOK, TOK)).T[:, 0:1]
    normed = (now * lax.rsqrt(total / D + EPS) * ngain[...]).astype(BF)
    xs[...] = dot(choose[0] + choose[1], normed, ((0,), (0,))).astype(BF).reshape(NS, 16, 256)

    here = lanes(x, 256)

    def block_rows(idx, cc):
        return pl.ds(pl.multiple_of((2 * idx + cc) * 16, 16), 16)

    keep = pltpu.make_async_copy(xs.at[me_s], x4.at[block_rows(0, c), here], loc_sem.at[5])
    keep.start()
    for idx, off in enumerate(ORDER):
        for j in (0, 1):
            if off == 0 and j == 0:
                continue
            to = at_z(-off, j)
            send(xs.at[to], x4.at[block_rows(idx, c), here], snd.at[4], x_sem.at[idx // 4], to, me_t)

    def chunk(k):
        return pl.ds(k * ROWS, ROWS)

    def stage_g(k):
        if k == 0:
            keep.wait()
            wait(x4.at[0:112, 0:256], x_sem.at[0])
        else:
            wait(x4.at[0:128, 0:256], x_sem.at[k])
        for i in (2, 1, 3):
            block = x4.at[chunk(k), here]
            send(block, block, snd.at[5], g_sem.at[k], me_s, t_of(y, x_peer(i)))

    def stage_m(k):
        wait(x4.at[chunk(k), 0:768], g_sem.at[k])
        if k == 0:
            local[0].wait()
            local[1].wait()
            for half in (0, 1):
                wait(wgu.at[:, 0:384], w_sem.at[2 + half])
        psend[chunk(k), :] = dot(x4[chunk(k), :], wgu[...]).astype(BF)
        for i in (2, 1, 3):
            to = y_peer(i)
            send(psend.at[chunk(k), lanes(to, 256)], precv.at[i - 1, chunk(k), :], snd.at[6], m_sem.at[k],
                 me_s, t_of(to, x))

    def stage_a(k):
        wait(precv.at[:, chunk(k), :], m_sem.at[k])
        both = psend[chunk(k), lanes(y, 256)].astype(F32)
        for i in range(3):
            both = both + precv[i, chunk(k), :].astype(F32)
        hid[chunk(k), lanes(y, 128)] = (silu(both[:, :128]) * both[:, 128:]).astype(BF)
        for i in (2, 1, 3):
            block = hid.at[chunk(k), lanes(y, 128)]
            send(block, block, snd.at[7], a_sem.at[k], me_s, t_of(y_peer(i), x))

    def stage_d(k):
        wait(hid.at[chunk(k), 0:384], a_sem.at[k])
        if k == 0:
            local[2].wait()
            wait(wd2.at[:, :, 0:768], w_sem.at[5])
        p2send[chunk(k), :] = dot(hid[chunk(k), :], wd2[...].reshape(512, 1024)).astype(BF)
        for i in (2, 1, 3):
            to = x_peer(i)
            send(p2send.at[chunk(k), lanes(to, 256)], p2recv.at[i - 1, chunk(k), :], snd.at[8], d_sem.at[k],
                 me_s, t_of(y, to))

    stay = pltpu.make_async_copy(rsend.at[block_rows(0, c)], ret.at[lanes(me_s, 16)], loc_sem.at[6])

    def stage_r(k):
        wait(p2recv.at[:, chunk(k), :], d_sem.at[k])
        done = p2send[chunk(k), lanes(x, 256)].astype(F32)
        for i in range(3):
            done = done + p2recv[i, chunk(k), :].astype(F32)
        rsend[chunk(k), :] = done.astype(BF)
        if k == 0:
            stay.start()
        for idx in range(4 * k, 4 * k + 4):
            for j in (0, 1):
                if idx == 0 and j == 0:
                    continue
                block = block_rows(idx, lax.rem(c + j, 2))
                send(rsend.at[block], ret.at[lanes(me_s, 16)], snd.at[9], r_sem.at[0], at_z(ORDER[idx], j), me_t)

    stages = (stage_g, stage_m, stage_a, stage_d, stage_r)
    for tick in range(NCH + len(stages) - 1):
        for n in reversed(range(len(stages))):
            if 0 <= tick - n < NCH:
                stages[n](tick - n)

    stay.wait()
    wait(ret.at[0:496], r_sem.at[0])
    back = ret[...]
    routed = rw[:, 0:1] * dot(choose[0], back) + rw[:, 1:2] * dot(choose[1], back)
    out[...] = (stream[...] + routed).astype(BF)

    wait(u_send.at[0 : NS - 1], u_sem.at[0])
    wait(e_send.at[0 : NS - 1], e_sem.at[0])
    wait(wo.at[:, 0:1984], snd.at[0])
    wait(ho.at[0, :, 0:768], snd.at[1])
    wait(ho.at[:, :, 0:1536], snd.at[2])
    wait(ss_recv.at[0 : NT - 1], snd.at[3])
    wait(xs.at[0 : NS - 1], snd.at[4])
    wait(x4.at[:, 0:768], snd.at[5])
    wait(psend.at[:, 0:768], snd.at[6])
    wait(hid.at[:, 0:384], snd.at[7])
    wait(p2send.at[:, 0:768], snd.at[8])
    wait(ret.at[0:496], snd.at[9])
    for half in (0, 1):
        wait(wgu.at[:, 0:384], w_sem.at[half])
    wait(wd2.at[:, :, 0:768], w_sem.at[4])


def per_device(
    residual, query_small, key_narrow_group, query_large, key_large, values, gates, log_decay,
    head_gain, out_weight, norm_gain, routes, route_weight, expert_gate, expert_up, expert_down,
):
    tab_i, tab_s = tables()
    vmem = pl.BlockSpec(memory_space=pltpu.VMEM)
    far = pl.BlockSpec(memory_space=pl.ANY)
    v = pltpu.VMEM
    dma = pltpu.SemaphoreType.DMA
    return pl.pallas_call(
        kernel,
        out_shape=jax.ShapeDtypeStruct((TOK, 256), BF),
        in_specs=[vmem] * 13 + [far] * 3 + [vmem] * 2,
        out_specs=vmem,
        scratch_shapes=[
            v((NS, 16, TOK), BF), v((NS, 16, TOK), BF), v((NS, 16, TOK), BF), v((NS, 16, TOK), BF),
            v((2, 2048, 256), BF), v((2, TOK, 2048), BF),
            v((1, TOK), F32), v((NT, 1, TOK), F32),
            v((TOK, 256), F32), v((2, TOK, 512), BF),
            v((NS, 16, 256), BF), v((512, 1024), BF), v((1024, 1024), BF), v((4, 128, 1024), BF),
            v((512, 1024), BF), v((3, 512, 256), BF), v((512, 512), BF),
            v((512, 1024), BF), v((3, 512, 256), BF), v((512, 256), BF), v((512, 256), BF),
            v((TOK, 512), BF), v((TOK, 512), BF), v((2, TOK, TOK), F32),
            dma((2, 8, 2)), dma((1,)), dma((2,)), dma((2,)), dma((4,)), dma((1,)), dma((NCH,)),
            dma((NCH,)), dma((NCH,)), dma((NCH,)), dma((NCH,)), dma((1,)),
            dma((6,)), dma((7,)), dma((10,)),
        ],
        compiler_params=pltpu.CompilerParams(collective_id=0, has_side_effects=True),
        name="layer",
    )(
        residual, query_small, key_narrow_group, query_large, key_large,
        values.reshape(TOK, 256), gates.reshape(TOK, 256), log_decay.reshape(TOK, 2),
        head_gain, out_weight, norm_gain.reshape(1, 256), routes, route_weight,
        expert_gate.reshape(4096, 128), expert_up.reshape(4096, 128),
        expert_down.reshape(4, 4, 128, 256), jnp.asarray(tab_i), jnp.asarray(tab_s),
    )


def solution(mesh):
    sp, tp = "sp", "tp"
    placed = (
        P(sp, tp), P(sp, tp), P(sp, tp), P(sp, tp), P(sp, tp),
        P(sp, None, tp), P(sp, None, tp), P(sp, None, tp),
        P(None, tp), P(None, sp, tp), P(tp), P(sp, None), P(sp, None),
        P(sp, None, tp), P(sp, None, tp), P(sp, None, tp),
    )
    return jax.shard_map(per_device, mesh=mesh, in_specs=placed, out_specs=P(sp, tp), check_vma=False)
```

time: 374 us -> 124 us (0.33)
  waiting for transfers between devices: 186 us -> 0 us
  Pallas kernels: 0 us -> 118 us
  blocking collectives: 91.8 us -> 0 us
  matrix products: 34.7 us -> 0 us
  starting transfers between devices: 22.2 us -> 0 us
  between operations: 20.9 us -> 0.02 us
  other arithmetic: 7.46 us -> 0 us
    all_gather x3 -> x0, waiting for transfers between devices: 163 us -> none  [the longest x1 63 us: gathered_once(): both, at, found = (lax.all_gather(jnp.concatenate(lines), axis), 0, {})]
    pallas_call x0 -> x1, Pallas kernels: none -> 118 us  [per_device(): pl.pallas_call(kernel, out_shape=jax.ShapeDtypeStruct((TOK, 256), BF), in...]
    all_to_all x2 -> x0, blocking collectives: 66.5 us -> none  [the longest x1 34.8 us: per_device(): lax.all_to_all(outgoing, SP, split_axis=0, concat_axis=0, tiled=True)]
    dot_general x13 -> x0, matrix products: 34.7 us -> none  [the longest x2 23.7 us: final_result(): jnp.einsum('ihd,hdv->ihv', rot_queries.astype(jnp.float32), state_in, pre...]
    all_to_all x2 -> x0, starting transfers between devices: 22.1 us -> none  [the longest x1 15.5 us: per_device(): lax.all_to_all(expert_out, SP, split_axis=0, concat_axis=0, tiled=True)]
    all_to_all x2 -> x0, waiting for transfers between devices: 22.1 us -> none  [the longest x1 22.1 us: per_device(): lax.all_to_all(expert_out, SP, split_axis=0, concat_axis=0, tiled=True)]
    psum x2 -> x0, blocking collectives: 16.8 us -> none  [by_axis(): return functools.reduce(lax.psum, axes, array)]
    all_gather x1 -> x0, blocking collectives: 8.56 us -> none  [gathered_once(): both, at, found = (lax.all_gather(jnp.concatenate(lines), axis), 0, {})]
  transfers between devices with their start and end apart: 5 -> 0, of which waited for: 4 -> 0; matrix products, arithmetic and copies ran while one was open for 8% -> 0% of each run, Pallas kernels for 0% -> 0%
where the time goes in v1:
time: 124 us; the launch traced here: 123 us
  Pallas kernels  118 us (95%)
  local copies, waits for them, and re-layouts  5.7 us (5%)
    pallas_call x1, Pallas kernels, per_device(): pl.pallas_call(kernel, out_shape=jax.ShapeDtypeStruct((TOK, 256), BF), in...  118 us
    unnamed x14, local copies, waits for them, and re-layouts  5.04 us

profile of v1, /device:TPU:1, one launch (start us, length us, event | category | flops | bytes accessed | tf_op | source)
XLA Modules:
  0.0 123.3 jit_solution(13578349942006928018)
XLA Ops:
  0.0 0.0 copy-start.2
  0.0 0.7 copy-done.2
  0.7 0.7 copy.19
  1.4 0.0 copy-start.3
  1.4 0.0 copy-start.4
  1.4 0.7 copy-done.3
  2.1 0.0 copy-start
  2.1 0.0 copy-start.1
  2.1 0.7 copy.20.routes
  2.8 0.0 copy-done.4
  2.8 0.7 copy.21.rw
  3.6 0.0 copy-done
  3.6 0.0 copy-done.1
  3.6 0.7 copy_bitcast_fusion
  4.2 117.6 %layer.1 = bf16[128,256]{1,0:T(8,128)(2,1)} custom-call(bf16[128,256]{1,0:T(8,128)(2,1)} %res.1, bf16[128,128]{1,0:T(8,128)(2,1)} %qs.1, bf16[128,128]{1,0:T(8,128)(2,1)} %ks.1, bf16[128,256]{1,0:T(8,128)(2,1)} %ql.1, bf16[128,256]{1,0:T(8,128)(2,1)} %kl.1, bf16[128,256]{1,0:T(8,128)(2,1)} %get-tuple-element.6.vals, ...), custom_call_target="tpu_custom_call" | custom-call | tf_op jit(solution)/shard_map/layer/pallas_call | solution.py:424
  121.9 1.5 %copy.27 = bf16[128,256]{1,0:T(8,128)(2,1)} copy(bf16[128,256]{1,0:T(8,128)(2,1)} %layer.1) | data formatting | bytes 131072
Async XLA Ops:
  0.0 0.7 copy-start.2
  1.4 0.7 copy-start.3
  1.4 1.4 %copy-start.4 = (f32[128,2]{0,1:T(2,128)S(1)}, f32[128,2]{0,1:T(2,128)}, u32[]{:S(2)}) copy-start(f32[128,2]{0,1:T(2,128)} %param.30) | copy-start | bytes 3076
  2.1 1.5 %copy-start = (bf16[128,2,128]{2,1,0:T(2,128)(2,1)S(1)}, bf16[128,2,128]{2,1,0:T(2,128)(2,1)}, u32[]{:S(2)}) copy-start(bf16[128,2,128]{2,1,0:T(2,128)(2,1)} %param.24) | copy-start | bytes 196612
  2.1 1.5 %copy-start.1 = (bf16[128,2,128]{2,1,0:T(2,128)(2,1)S(1)}, bf16[128,2,128]{2,1,0:T(2,128)(2,1)}, u32[]{:S(2)}) copy-start(bf16[128,2,128]{2,1,0:T(2,128)(2,1)} %param.23) | copy-start | bytes 196612
